TPU v7x, 32 devices: a whole 2x2x4 slice. The times are simulated.
32 devices in a mesh: ep: 8 (over z, core), tp: 4 (over y, x).
Axes of the slice: x: 2, y: 2, z: 4, core: 2. Of those that a mesh axis runs over, the one named last changes fastest.
Arguments:
- tokens: bfloat16 [128, 2048], P('ep'), may hold values from -6 to 6
- old_state: float32 [128, 16, 128, 128], P('ep', 'tp'), may hold values from -2 to 2
- lower_bound: float32 [2048], P('tp'), may hold values from 0.05 to 0.95
- head_gain: float32 [2048], P('tp'), may hold values from 0.1 to 1.9
- norm_gains: float32 [4, 2048], replicated, may hold values from 0.1 to 1.9
- w_query: bfloat16 [2048, 2048], P('ep', 'tp'), may hold values from -0.125 to 0.125
- w_forget: bfloat16 [2048, 2048], P('ep', 'tp'), may hold values from -0.125 to 0.125
- w_value: bfloat16 [2048, 2048], P('ep', 'tp'), may hold values from -0.125 to 0.125
- w_outgate: bfloat16 [2048, 2048], P('ep', 'tp'), may hold values from -0.125 to 0.125
- w_mix_out: bfloat16 [2048, 2048], P('tp', 'ep'), may hold values from -0.125 to 0.125
- routes: int32 [128, 2], P('ep'), may hold values from 0 to 7, all different within a row; in each aligned block of 16 rows (0 to 15, 16 to 31, ...) at most 8 rows name the same one
- route_scores: float32 [128, 2], P('ep'), may hold values from -6 to 6
- w_exp_gate: bfloat16 [8, 2048, 3584], P('ep', None, 'tp'), may hold values from -0.125 to 0.125
- w_exp_up: bfloat16 [8, 2048, 3584], P('ep', None, 'tp'), may hold values from -0.125 to 0.125
- w_exp_down: bfloat16 [8, 3584, 2048], P('ep', 'tp'), may hold values from -0.75 to 0.75
- w_dense_gate: bfloat16 [2048, 6144], P('ep', 'tp'), may hold values from -0.125 to 0.125
- w_dense_up: bfloat16 [2048, 6144], P('ep', 'tp'), may hold values from -0.125 to 0.125
- w_dense_down: bfloat16 [6144, 2048], P('tp', 'ep'), may hold values from -0.75 to 0.75
- dense_mix: bfloat16 [2048], replicated, may hold values from -0.125 to 0.125
Outputs:
- layer_out: bfloat16 [128, 2048], P('ep', 'tp')
- new_state: float32 [128, 16, 128, 128], P('ep', 'tp')
Inputs may be any that keep to these rules, and one draw needn't show every extreme that they name: `routes`: each row names 2 different experts. In each aligned block of 16 rows no expert is named by more than 8 rows, and in every draw some expert is named by exactly 8 rows of some block.
All inputs are finite; a program needn't handle non-finite values.
Results may differ from a plain program's by a relative error of at most 0.025.
Values may be sent and summed in bfloat16 or wider, within the bound.
No kernel may reach another device: no remote copies, remote signals or barrier semaphores. Data moves between devices by JAX's collectives and lax.ppermute only.
A program may use at most 64 MiB of HBM per device.

v0:
```python
import jax
import jax.numpy as jnp
from jax import lax
from jax.sharding import PartitionSpec as P

EPS = 1e-06


def rms_scale(values):
    return lax.rsqrt(jnp.mean(values * values, axis=-1, keepdims=True) + EPS)


def body(
    tokens,
    old_state,
    lower_bound,
    head_gain,
    norm_gains,
    w_query,
    w_forget,
    w_value,
    w_outgate,
    w_mix_out,
    routes,
    route_scores,
    w_exp_gate,
    w_exp_up,
    w_exp_down,
    w_dense_gate,
    w_dense_up,
    w_dense_down,
    dense_mix,
):
    highest = lax.Precision.HIGHEST
    seqs, width = tokens.shape
    column_index = lax.axis_index("tp")
    part_width = width // lax.axis_size("tp")
    resid = tokens.astype(jnp.float32)
    normed = (resid * rms_scale(resid) * norm_gains[0]).astype(jnp.bfloat16)
    in_weights = jnp.concatenate([w_query, w_forget, w_value, w_outgate], axis=1)
    mix_rows = lax.all_to_all(normed, "ep", split_axis=1, concat_axis=0, tiled=True)
    projected = lax.psum_scatter(
        jnp.dot(mix_rows, in_weights, preferred_element_type=jnp.float32).astype(jnp.bfloat16),
        "ep",
        scatter_dimension=0,
        tiled=True,
    ).astype(jnp.float32)
    query_raw, forget_raw, value, out_gate = jnp.split(projected, 4, axis=1)
    heads = old_state.shape[1]
    head_size = old_state.shape[2]
    shape_heads = (seqs, heads, head_size)
    forget = lower_bound + (1.0 - lower_bound) * jax.nn.sigmoid(forget_raw)
    key_in = (1.0 - lower_bound) * jax.nn.sigmoid(-forget_raw)
    new_state = forget.reshape(shape_heads)[..., None] * old_state + key_in.reshape(shape_heads)[
        ..., None
    ] * value.reshape(seqs, heads, 1, head_size)
    query = jax.nn.silu(query_raw).reshape(shape_heads)
    read = jnp.einsum("thk,thkv->thv", query, new_state, precision=highest)
    gated = (
        read
        * rms_scale(read)
        * head_gain.reshape(heads, head_size)
        * jax.nn.silu(out_gate).reshape(shape_heads)
    )
    mixed_heads = gated.reshape(seqs, heads * head_size).astype(jnp.bfloat16)
    mix_part = jnp.dot(
        mixed_heads,
        lax.all_gather(w_mix_out, "ep", axis=1, tiled=True),
        preferred_element_type=jnp.float32,
    ).astype(jnp.bfloat16)
    mix_part = lax.optimization_barrier(mix_part).astype(jnp.float32)
    mix_out = lax.psum(mix_part.astype(jnp.bfloat16), "tp")
    mix_wide = lax.optimization_barrier(mix_out).astype(jnp.float32)
    after_mix = resid + mix_wide * rms_scale(mix_wide) * norm_gains[1]
    ffn_in = (after_mix * rms_scale(after_mix) * norm_gains[2]).astype(jnp.bfloat16)
    experts = lax.axis_size("ep")
    topk = routes.shape[1]
    capacity = max(2, 2 * seqs * topk // experts)
    flat_routes = routes.reshape(-1)
    onehot = (flat_routes[:, None] == jnp.arange(experts, dtype=jnp.int32)[None, :]).astype(
        jnp.int32
    )
    before = jnp.cumsum(onehot, axis=0) - onehot
    slots = jnp.sum(onehot * before, axis=1)
    cells = flat_routes * capacity + slots
    placed = cells[None, :] == jnp.arange(experts * capacity, dtype=jnp.int32)[:, None]
    repeated = jnp.repeat(ffn_in, topk, axis=0)
    outgoing = jnp.dot(placed.astype(jnp.bfloat16), repeated, preferred_element_type=jnp.float32)
    outgoing = outgoing.astype(jnp.bfloat16).reshape(experts, capacity, width)
    arrived = lax.all_to_all(outgoing, "ep", split_axis=0, concat_axis=0, tiled=True)
    sources, items, _ = arrived.shape
    expert_rows = arrived.reshape(sources * items, width)
    gate_pre = jnp.dot(expert_rows, w_exp_gate[0], preferred_element_type=jnp.float32)
    up_pre = jnp.dot(expert_rows, w_exp_up[0], preferred_element_type=jnp.float32)
    hidden = (jax.nn.silu(gate_pre) * up_pre).astype(jnp.bfloat16)
    partial_rows = jnp.dot(hidden, w_exp_down[0], preferred_element_type=jnp.float32).astype(
        jnp.bfloat16
    )
    partial_rows = lax.optimization_barrier(partial_rows).astype(jnp.float32)
    partial_rows = partial_rows.reshape(sources, items, width)
    summed = lax.psum_scatter(
        partial_rows.astype(jnp.bfloat16), "tp", scatter_dimension=2, tiled=True
    )
    returned = lax.all_to_all(summed, "ep", split_axis=0, concat_axis=0, tiled=True)
    first = jax.nn.sigmoid(route_scores[:, 0] - route_scores[:, 1])
    second = jax.nn.sigmoid(route_scores[:, 1] - route_scores[:, 0])
    route_weight = jnp.stack([first, second], axis=1).reshape(-1)
    weight_table = jnp.sum(
        (placed.astype(jnp.float32) * route_weight[None, :]).reshape(
            experts * capacity, seqs, topk
        ),
        axis=2,
    )
    expert_sum = jnp.dot(
        weight_table.T,
        returned.reshape(experts * capacity, part_width).astype(jnp.float32),
        precision=highest,
    )
    dense_weights = jnp.concatenate([w_dense_gate, w_dense_up], axis=1)
    dense_rows = lax.all_to_all(ffn_in, "ep", split_axis=1, concat_axis=0, tiled=True)
    dense_pre = lax.psum_scatter(
        jnp.dot(dense_rows, dense_weights, preferred_element_type=jnp.float32).astype(jnp.bfloat16),
        "ep",
        scatter_dimension=0,
        tiled=True,
    ).astype(jnp.float32)
    dense_gate_pre, dense_up_pre = jnp.split(dense_pre, 2, axis=1)
    dense_hidden = (jax.nn.silu(dense_gate_pre) * dense_up_pre).astype(jnp.bfloat16)
    dense_partial = jnp.dot(
        dense_hidden,
        lax.all_gather(w_dense_down, "ep", axis=1, tiled=True),
        preferred_element_type=jnp.float32,
    )
    dense_out = lax.psum_scatter(
        dense_partial.astype(jnp.bfloat16), "tp", scatter_dimension=1, tiled=True
    ).astype(jnp.float32)
    mix_weight = jax.nn.sigmoid(jnp.dot(ffn_in, dense_mix, preferred_element_type=jnp.float32))
    ffn_out = expert_sum + mix_weight[:, None] * dense_out
    squares = lax.psum(jnp.sum(ffn_out * ffn_out, axis=1), "tp")
    out_scale = lax.rsqrt(squares / width + EPS)
    gain_part = lax.dynamic_slice_in_dim(norm_gains[3], column_index * part_width, part_width, 0)
    resid_part = lax.dynamic_slice_in_dim(after_mix, column_index * part_width, part_width, 1)
    layer_out = (resid_part + ffn_out * out_scale[:, None] * gain_part).astype(jnp.bfloat16)
    return (layer_out, new_state)


def solution(mesh):
    return jax.shard_map(
        body,
        mesh=mesh,
        in_specs=(
            P("ep", None),
            P("ep", "tp", None, None),
            P("tp"),
            P("tp"),
            P(),
            P("ep", "tp"),
            P("ep", "tp"),
            P("ep", "tp"),
            P("ep", "tp"),
            P("tp", "ep"),
            P("ep", None),
            P("ep", None),
            P("ep", None, "tp"),
            P("ep", None, "tp"),
            P("ep", "tp", None),
            P("ep", "tp"),
            P("ep", "tp"),
            P("tp", "ep"),
            P(),
        ),
        out_specs=(P("ep", "tp"), P("ep", "tp", None, None)),
        check_vma=False,
    )
```

profile of v0, /device:TPU:0, one launch (start us, length us, event | category | flops | bytes accessed | tf_op | source)
XLA Modules:
  0.0 319.4 jit_solution(3477213161517081613)
XLA Ops:
  7.2 0.9 fusion.58
  8.2 1.0 fusion.42
  9.2 0.9 fusion.44
  10.1 12.1 %all_to_all.48 = bf16[16,8,256]{2,0,1:T(8,128)(2,1)S(1)} all-to-all(bf16[16,8,256]{2,0,1:T(8,128)(2,1)S(1)} %bitcast.82), channel_id=1, replica_groups=mesh['ep'=8,'tp'=4] {'ep'}, dimensions={1} | all-to-all | bytes 131072 | tf_op jit(solution)/shard_map/all_to_all | solution.py:41
  22.2 2.3 convolution_convert_fusion.1
  24.5 0.7 all-gather.3.cloned.1.call-update
  25.3 0.1 copy.38
  25.4 0.1 eq.35
  25.5 0.1 fusion.53
  25.5 0.1 reduce_window_sum.11
  25.6 0.2 select_reduce_fusion.1
  25.8 28.7 %reduce-scatter.5.cloned.1.call-done = bf16[16,2048]{1,0:T(8,128)(2,1)} async-done(((bf16[128,2048]{1,0:T(8,128)(2,1)}), bf16[16,2048]{1,0:T(8,128)(2,1)}) %reduce-scatter.5.cloned.1.call-update) | async-done | bytes 65552 | tf_op jit(solution)/shard_map/reduce_scatter | solution.py:42
  54.5 0.8 convert_element_type.70
  55.4 0.7 split.26
  56.2 4.4 %multiply_add_fusion = f32[16,4,128,128]{3,2,1,0:T(8,128)S(1)} fusion(f32[16,4,128,128]{3,2,1,0:T(8,128)} %param.20, f32[16,4,128]{2,1,0:T(4,128)S(1)} %mul.223, f32[16,4,128]{2,1,0:T(4,128)S(1)} %mul.221, f32[16,4,128]{2,1,0:T(4,128)S(1)} %mul.217), kind=kLoop, calls=%fused_computation | loop fusion | flops 3145728 | bytes 8486912 | tf_op jit(solution)/shard_map/add | solution.py:54
  60.7 2.0 copy-done
  62.6 3.7 %fusion.59 = f32[16,4,1,128]{3,2,1,0:T(1,128)S(1)} fusion(f32[16,4,128,1]{2,3,1,0:T(1,128)S(1)} %bitcast.84, f32[16,4,128,128]{3,2,1,0:T(8,128)S(1)} %multiply_add_fusion), kind=kOutput, calls=%fused_computation.92 | convolution fusion | flops 12582912 | bytes 4259840 | tf_op jit(solution)/shard_map/thk,thkv->thv/dot_general | solution.py:58
  66.3 0.1 multiply_reduce_fusion.2
  66.4 0.1 multiply_convert_fusion.1
  66.5 18.5 %all-gather.3.cloned.1.call-done = bf16[512,2048]{1,0:T(8,128)(2,1)} async-done(((bf16[512,256]{1,0:T(8,128)(2,1)}), bf16[512,2048]{1,0:T(8,128)(2,1)}) %all-gather.3.cloned.1.call-update) | async-done | bytes 2097168 | tf_op jit(solution)/shard_map/all_gather | solution.py:68
  85.0 2.6 convolution_convert_fusion.4
  87.7 41.1 %all-reduce.2.cloned.1.call-done = bf16[16,2048]{1,0:T(8,128)(2,1)} async-done(((bf16[16,2048]{1,0:T(8,128)(2,1)}), bf16[16,2048]{1,0:T(8,128)(2,1)}) %all-reduce.2.cloned.1.call-update) | async-done | bytes 65552 | tf_op jit(solution)/shard_map/psum | solution.py:72
  128.8 1.0 fusion.40
  129.7 1.0 multiply_reduce_fusion
  130.8 0.1 multiply_convert_fusion
  130.9 0.1 broadcast_in_dim.2
  131.0 0.1 reshape.103
  131.0 0.2 fusion.9
  131.2 14.1 %all_to_all.49 = bf16[8,8,2048]{2,1,0:T(8,128)(2,1)S(1)} all-to-all(bf16[8,8,2048]{2,1,0:T(8,128)(2,1)S(1)} %fusion.9), channel_id=1, replica_groups=mesh['ep'=8,'tp'=4] {'ep'}, dimensions={0} | all-to-all | bytes 524288 | tf_op jit(solution)/shard_map/all_to_all | solution.py:90
  145.4 2.7 fusion.4
  148.1 5.5 %fusion.6 = bf16[64,2048]{1,0:T(8,128)(2,1)} fusion(bf16[1,896,2048]{2,1,0:T(8,128)(2,1)} %param.33, bf16[1,2048,896]{2,1,0:T(8,128)(2,1)} %param.32, bf16[8,8,2048]{2,1,0:T(8,128)(2,1)S(1)} %all_to_all.49, f32[64,896]{1,0:T(8,128)S(1)} %fusion.4), kind=kOutput, calls=%fused_computation.9 | convolution fusion | flops 470237184 | bytes 8093696 | tf_op jit(solution)/shard_map/dot_general | solution.py:96
  153.7 8.3 %all_to_all.50 = bf16[16,8,256]{2,0,1:T(8,128)(2,1)S(1)} all-to-all(bf16[16,8,256]{2,0,1:T(8,128)(2,1)S(1)} %bitcast.83), channel_id=1, replica_groups=mesh['ep'=8,'tp'=4] {'ep'}, dimensions={1} | all-to-all | bytes 131072 | tf_op jit(solution)/shard_map/all_to_all | solution.py:120
  162.0 1.3 convolution_convert_fusion
  163.4 0.5 all-gather.5.cloned.1.call-update
  163.9 0.1 reduce_sum.69
  164.0 0.1 copy.39
  164.2 0.1 select_reduce_fusion
  164.2 11.9 %reduce-scatter.7.cloned.1.call-done = bf16[8,8,512]{2,1,0:T(8,128)(2,1)} async-done(((bf16[8,8,2048]{2,1,0:T(8,128)(2,1)}), bf16[8,8,512]{2,1,0:T(8,128)(2,1)}) %reduce-scatter.7.cloned.1.call-update) | async-done | bytes 65552 | tf_op jit(solution)/shard_map/reduce_scatter | solution.py:101
  176.1 4.6 %all-to-all-start.2 = ((bf16[8,8,512]{2,1,0:T(8,128)(2,1)}), bf16[8,8,512]{2,1,0:T(8,128)(2,1)S(1)}, u32[]{:S(2)}, u32[]{:S(2)}) async-start(bf16[8,8,512]{2,1,0:T(8,128)(2,1)} %reduce-scatter.7.cloned.1.call-done), calls=%async_computation.4 | async-start | bytes 131072 | tf_op jit(solution)/shard_map/all_to_all | solution.py:104
  180.8 29.5 %reduce-scatter.9.cloned.1.call-done = bf16[16,3072]{1,0:T(8,128)(2,1)} async-done(((bf16[128,3072]{1,0:T(8,128)(2,1)}), bf16[16,3072]{1,0:T(8,128)(2,1)}) %reduce-scatter.9.cloned.1.call-update) | async-done | bytes 98320 | tf_op jit(solution)/shard_map/reduce_scatter | solution.py:121
  210.3 0.9 convert_element_type.82
  211.2 63.9 %all-gather.5.cloned.1.call-done = bf16[1536,2048]{1,0:T(8,128)(2,1)} async-done(((bf16[1536,256]{1,0:T(8,128)(2,1)}), bf16[1536,2048]{1,0:T(8,128)(2,1)}) %all-gather.5.cloned.1.call-update) | async-done | bytes 6291472 | tf_op jit(solution)/shard_map/all_gather | solution.py:131
  275.1 4.3 %convolution_convert_fusion.3 = bf16[16,2048]{1,0:T(8,128)(2,1)} fusion(bf16[1536,2048]{1,0:T(8,128)(2,1)} %all-gather.5.cloned.1.call-done, f32[16,3072]{1,0:T(8,128)S(1)} %convert_element_type.82), kind=kOutput, calls=%fused_computation.12 | convolution fusion | flops 100843520 | bytes 6553600 | tf_op jit(solution)/shard_map/dot_general | solution.py:129
  279.5 0.1 fusion.22
  279.6 22.3 %reduce-scatter.11.cloned.1.call-done = bf16[16,512]{1,0:T(8,128)(2,1)} async-done(((bf16[16,2048]{1,0:T(8,128)(2,1)}), bf16[16,512]{1,0:T(8,128)(2,1)}) %reduce-scatter.11.cloned.1.call-update) | async-done | bytes 16400 | tf_op jit(solution)/shard_map/reduce_scatter | solution.py:134
  301.9 1.0 multiply_reduce_fusion.1
  302.9 8.9 %psum.15 = f32[16]{0:T(128)S(1)} all-reduce(f32[16]{0:T(128)S(1)} %get-tuple-element.14), channel_id=1, replica_groups=mesh['ep'=8,'tp'=4] {'tp'}, use_global_device_ids=true, to_apply=%region_13.14 | all-reduce | flops 16 | bytes 128 | tf_op jit(solution)/shard_map/psum | solution.py:139
  311.8 0.7 add_convert_fusion
  (50 shorter events, 0.6 us)
Async XLA Ops:
  7.2 18.1 %copy-start.4 = (s32[16,2]{0,1:T(2,128)S(1)}, s32[16,2]{0,1:T(2,128)}, u32[]{:S(2)}) copy-start(s32[16,2]{0,1:T(2,128)} %param.29) | copy-start | bytes 388
  7.2 18.6 %copy-start.2 = (f32[512]{0:T(512)S(1)}, f32[512]{0:T(512)}, u32[]{:S(2)}) copy-start(f32[512]{0:T(512)} %param.21) | copy-start | bytes 6148
  7.2 47.3 %reduce-scatter.5.cloned.1.call-start = ((), (), s32[]{:S(2)}) async-start(), calls=%async_computation.8 | async-start | bytes 589824 | tf_op jit(solution)/shard_map/reduce_scatter | solution.py:42
  24.5 60.5 %all-gather.3.cloned.1.call-start = ((), (), s32[]{:S(2)}) async-start(), calls=%async_computation.9 | async-start | bytes 2359296 | tf_op jit(solution)/shard_map/all_gather | solution.py:68
  25.2 103.5 %all-reduce.2.cloned.1.call-start = ((), (), s32[]{:S(2)}) async-start(), calls=%async_computation.10 | async-start | bytes 131072 | tf_op jit(solution)/shard_map/psum | solution.py:72
  60.6 2.0 copy-start
  60.6 5.8 %copy-start.5 = (f32[512]{0:T(512)S(1)}, f32[512]{0:T(512)}, u32[]{:S(2)}) copy-start(f32[512]{0:T(512)} %param.22) | copy-start | bytes 6148
  60.6 69.1 %copy-start.1 = (bf16[16,2048]{1,0:T(8,128)(2,1)S(1)}, bf16[16,2048]{1,0:T(8,128)(2,1)}, u32[]{:S(2)}) copy-start(bf16[16,2048]{1,0:T(8,128)(2,1)} %param.19) | copy-start | bytes 196612
  87.6 88.5 %reduce-scatter.7.cloned.1.call-start = ((), (), s32[]{:S(2)}) async-start(), calls=%async_computation.11 | async-start | bytes 327680 | tf_op jit(solution)/shard_map/reduce_scatter | solution.py:101
  148.1 13.9 %copy-start.7 = (bf16[256,1536]{1,0:T(8,128)(2,1)S(1)}, bf16[256,1536]{1,0:T(8,128)(2,1)}, u32[]{:S(2)}) copy-start(bf16[256,1536]{1,0:T(8,128)(2,1)} %param.35) | copy-start | bytes 2359300
  148.1 13.9 %copy-start.8 = (bf16[256,1536]{1,0:T(8,128)(2,1)S(1)}, bf16[256,1536]{1,0:T(8,128)(2,1)}, u32[]{:S(2)}) copy-start(bf16[256,1536]{1,0:T(8,128)(2,1)} %param.34) | copy-start | bytes 2359300
  153.6 10.3 %copy-start.3 = (bf16[2048]{0:T(1024)(128)(2,1)S(1)}, bf16[2048]{0:T(1024)(128)(2,1)}, u32[]{:S(2)}) copy-start(bf16[2048]{0:T(1024)(128)(2,1)} %param.37) | copy-start | bytes 12292
  153.6 10.5 %copy-start.6 = (f32[16,2]{0,1:T(2,128)S(1)}, f32[16,2]{0,1:T(2,128)}, u32[]{:S(2)}) copy-start(f32[16,2]{0,1:T(2,128)} %param.30) | copy-start | bytes 388
  153.7 56.6 %reduce-scatter.9.cloned.1.call-start = ((), (), s32[]{:S(2)}) async-start(), calls=%async_computation.12 | async-start | bytes 884736 | tf_op jit(solution)/shard_map/reduce_scatter | solution.py:121
  163.3 111.8 %all-gather.5.cloned.1.call-start = ((), (), s32[]{:S(2)}) async-start(), calls=%async_computation.13 | async-start | bytes 7077888 | tf_op jit(solution)/shard_map/all_gather | solution.py:131
  176.1 103.5 %all-to-all-start.2 = ((bf16[8,8,512]{2,1,0:T(8,128)(2,1)}), bf16[8,8,512]{2,1,0:T(8,128)(2,1)S(1)}, u32[]{:S(2)}, u32[]{:S(2)}) async-start(bf16[8,8,512]{2,1,0:T(8,128)(2,1)} %reduce-scatter.7.cloned.1.call-done), calls=%async_computation.4 | async-start | bytes 131072 | tf_op jit(solution)/shard_map/all_to_all | solution.py:104
  180.7 121.2 %reduce-scatter.11.cloned.1.call-start = ((), (), s32[]{:S(2)}) async-start(), calls=%async_computation.14 | async-start | bytes 81920 | tf_op jit(solution)/shard_map/reduce_scatter | solution.py:134
Sparse Core Ops, SparseCore 0:
  24.6 29.8 reduce-scatter.4
  56.1 28.8 all-gather.2
  87.9 40.8 all-reduce.1
  153.8 22.2 reduce-scatter.6
  178.2 31.9 reduce-scatter.8
  211.7 63.3 all-gather.4
  279.6 22.2 reduce-scatter.10
where the time goes:
time: 320 us; the launch traced here: 319 us
  waiting for transfers between devices  217 us (68%)
  blocking collectives  43.4 us (14%)
  matrix products  23.7 us (7%)
  between operations  14.4 us (4%)
  other arithmetic  11.5 us (4%)
  starting transfers between devices  4.89 us (2%)
  local copies, waits for them, and re-layouts  4.25 us (1%)
    all_gather x1, waiting for transfers between devices, body(): lax.all_gather(w_dense_down, 'ep', axis=1, tiled=True)  63.9 us
    psum x1, waiting for transfers between devices, body(): mix_out = lax.psum(mix_part.astype(jnp.bfloat16), 'tp')  41.1 us
    reduce_scatter x1, waiting for transfers between devices, body(): lax.psum_scatter(jnp.dot(dense_rows, dense_weights, preferred_element_typ...  29.5 us
    reduce_scatter x1, waiting for transfers between devices, body(): lax.psum_scatter(jnp.dot(mix_rows, in_weights, preferred_element_type=jnp...  28.7 us
    reduce_scatter x1, waiting for transfers between devices, body(): lax.psum_scatter(dense_partial.astype(jnp.bfloat16), 'tp', scatter_dimens...  22.3 us
    all_gather x1, waiting for transfers between devices, body(): lax.all_gather(w_mix_out, 'ep', axis=1, tiled=True)  18.5 us
    all_to_all x1, blocking collectives, body(): lax.all_to_all(outgoing, 'ep', split_axis=0, concat_axis=0, tiled=True)  14.1 us
    all_to_all x1, blocking collectives, body(): lax.all_to_all(normed, 'ep', split_axis=1, concat_axis=0, tiled=True)  12.1 us
  transfers between devices with their start and end apart: 8, of which 7 were waited for; matrix products, arithmetic and copies ran while one was open for 5% of the time, Pallas kernels for 0%

commit v1 on v0

--- a/solution.py
+++ b/solution.py
@@ -126,10 +126,9 @@
     ).astype(jnp.float32)
     dense_gate_pre, dense_up_pre = jnp.split(dense_pre, 2, axis=1)
     dense_hidden = (jax.nn.silu(dense_gate_pre) * dense_up_pre).astype(jnp.bfloat16)
+    _produce_spot = lambda u_in: jnp.concatenate(jax.lax.all_gather(u_in, "ep"), 1)
     dense_partial = jnp.dot(
-        dense_hidden,
-        lax.all_gather(w_dense_down, "ep", axis=1, tiled=True),
-        preferred_element_type=jnp.float32,
+        dense_hidden, _produce_spot(w_dense_down), preferred_element_type=jnp.float32
     )
     dense_out = lax.psum_scatter(
         dense_partial.astype(jnp.bfloat16), "tp", scatter_dimension=1, tiled=True

time: 320 us -> 330 us (1.031)
  local copies, waits for them, and re-layouts: 4.25 us -> 12.9 us
    reshape x0 -> x1, local copies, waits for them, and re-layouts: none -> 8.63 us  [body(): jnp.concatenate(jax.lax.all_gather(u_in, 'ep'), 1)]
  transfers between devices with their start and end apart: 8 -> 8, of which waited for: 7 -> 7; matrix products, arithmetic and copies ran while one was open for 5% -> 8% of each run, Pallas kernels for 0% -> 0%
where the time goes in v1:
time: 330 us; the launch traced here: 329 us
  waiting for transfers between devices  217 us (66%)
  blocking collectives  43.4 us (13%)
  matrix products  24.5 us (7%)
  between operations  14.4 us (4%)
  local copies, waits for them, and re-layouts  12.9 us (4%)
  other arithmetic  11.5 us (3%)
  starting transfers between devices  4.89 us (1%)
    all_gather x1, waiting for transfers between devices, body(): jax.lax.all_gather(u_in, 'ep')  63.5 us
    psum x1, waiting for transfers between devices, body(): mix_out = lax.psum(mix_part.astype(jnp.bfloat16), 'tp')  41.1 us
    reduce_scatter x1, waiting for transfers between devices, body(): lax.psum_scatter(jnp.dot(dense_rows, dense_weights, preferred_element_typ...  29.5 us
    reduce_scatter x1, waiting for transfers between devices, body(): lax.psum_scatter(jnp.dot(mix_rows, in_weights, preferred_element_type=jnp...  28.7 us
    reduce_scatter x1, waiting for transfers between devices, body(): lax.psum_scatter(dense_partial.astype(jnp.bfloat16), 'tp', scatter_dimens...  22.8 us
    all_gather x1, waiting for transfers between devices, body(): lax.all_gather(w_mix_out, 'ep', axis=1, tiled=True)  18.5 us
    all_to_all x1, blocking collectives, body(): lax.all_to_all(outgoing, 'ep', split_axis=0, concat_axis=0, tiled=True)  14.1 us
    all_to_all x1, blocking collectives, body(): lax.all_to_all(normed, 'ep', split_axis=1, concat_axis=0, tiled=True)  12.1 us
  transfers between devices with their start and end apart: 8, of which 7 were waited for; matrix products, arithmetic and copies ran while one was open for 8% of the time, Pallas kernels for 0%

profile of v1, /device:TPU:0, one launch (start us, length us, event | category | flops | bytes accessed | tf_op | source)
XLA Modules:
  0.0 328.9 jit_solution(9589377973796641024)
XLA Ops:
  7.2 0.9 fusion.58
  8.2 1.0 fusion.42
  9.2 0.9 fusion.44
  10.1 12.1 %all_to_all.48 = bf16[16,8,256]{2,0,1:T(8,128)(2,1)S(1)} all-to-all(bf16[16,8,256]{2,0,1:T(8,128)(2,1)S(1)} %bitcast.88), channel_id=1, replica_groups=mesh['ep'=8,'tp'=4] {'ep'}, dimensions={1} | all-to-all | bytes 131072 | tf_op jit(solution)/shard_map/all_to_all | solution.py:41
  22.2 2.3 convolution_convert_fusion.1
  24.5 0.7 all-gather.4.cloned.1.call-update
  25.3 0.1 copy.46
  25.4 0.1 eq.35
  25.5 0.1 fusion.53
  25.5 0.1 reduce_window_sum.11
  25.6 0.2 select_reduce_fusion.1
  25.8 28.7 %reduce-scatter.5.cloned.1.call-done = bf16[16,2048]{1,0:T(8,128)(2,1)} async-done(((bf16[128,2048]{1,0:T(8,128)(2,1)}), bf16[16,2048]{1,0:T(8,128)(2,1)}) %reduce-scatter.5.cloned.1.call-update) | async-done | bytes 65552 | tf_op jit(solution)/shard_map/reduce_scatter | solution.py:42
  54.5 0.8 convert_element_type.70
  55.4 0.7 split.26
  56.2 4.4 %multiply_add_fusion = f32[16,4,128,128]{3,2,1,0:T(8,128)S(1)} fusion(f32[16,4,128,128]{3,2,1,0:T(8,128)} %param.20, f32[16,4,128]{2,1,0:T(4,128)S(1)} %mul.223, f32[16,4,128]{2,1,0:T(4,128)S(1)} %mul.221, f32[16,4,128]{2,1,0:T(4,128)S(1)} %mul.217), kind=kLoop, calls=%fused_computation | loop fusion | flops 3145728 | bytes 8486912 | tf_op jit(solution)/shard_map/add | solution.py:54
  60.7 2.0 copy-done
  62.6 3.7 %fusion.59 = f32[16,4,1,128]{3,2,1,0:T(1,128)S(1)} fusion(f32[16,4,128,1]{2,3,1,0:T(1,128)S(1)} %bitcast.90, f32[16,4,128,128]{3,2,1,0:T(8,128)S(1)} %multiply_add_fusion), kind=kOutput, calls=%fused_computation.92 | convolution fusion | flops 12582912 | bytes 4259840 | tf_op jit(solution)/shard_map/thk,thkv->thv/dot_general | solution.py:58
  66.3 0.1 multiply_reduce_fusion.2
  66.4 0.1 multiply_convert_fusion.1
  66.5 18.5 %all-gather.4.cloned.1.call-done = bf16[512,2048]{1,0:T(8,128)(2,1)} async-done(((bf16[512,256]{1,0:T(8,128)(2,1)}), bf16[512,2048]{1,0:T(8,128)(2,1)}) %all-gather.4.cloned.1.call-update) | async-done | bytes 2097168 | tf_op jit(solution)/shard_map/all_gather | solution.py:68
  85.0 2.6 convolution_convert_fusion.4
  87.7 41.1 %all-reduce.2.cloned.1.call-done = bf16[16,2048]{1,0:T(8,128)(2,1)} async-done(((bf16[16,2048]{1,0:T(8,128)(2,1)}), bf16[16,2048]{1,0:T(8,128)(2,1)}) %all-reduce.2.cloned.1.call-update) | async-done | bytes 65552 | tf_op jit(solution)/shard_map/psum | solution.py:72
  128.8 1.0 fusion.40
  129.7 1.0 multiply_reduce_fusion
  130.8 0.1 multiply_convert_fusion
  130.9 0.1 broadcast_in_dim.2
  131.0 0.2 fusion.9
  131.2 14.1 %all_to_all.49 = bf16[8,8,2048]{2,1,0:T(8,128)(2,1)S(1)} all-to-all(bf16[8,8,2048]{2,1,0:T(8,128)(2,1)S(1)} %fusion.9), channel_id=1, replica_groups=mesh['ep'=8,'tp'=4] {'ep'}, dimensions={0} | all-to-all | bytes 524288 | tf_op jit(solution)/shard_map/all_to_all | solution.py:90
  145.4 2.7 fusion.4
  148.1 5.5 %fusion.6 = bf16[64,2048]{1,0:T(8,128)(2,1)} fusion(bf16[1,896,2048]{2,1,0:T(8,128)(2,1)} %param.33, bf16[1,2048,896]{2,1,0:T(8,128)(2,1)} %param.32, bf16[8,8,2048]{2,1,0:T(8,128)(2,1)S(1)} %all_to_all.49, f32[64,896]{1,0:T(8,128)S(1)} %fusion.4), kind=kOutput, calls=%fused_computation.9 | convolution fusion | flops 470237184 | bytes 8093696 | tf_op jit(solution)/shard_map/dot_general | solution.py:96
  153.7 8.3 %all_to_all.50 = bf16[16,8,256]{2,0,1:T(8,128)(2,1)S(1)} all-to-all(bf16[16,8,256]{2,0,1:T(8,128)(2,1)S(1)} %bitcast.89), channel_id=1, replica_groups=mesh['ep'=8,'tp'=4] {'ep'}, dimensions={1} | all-to-all | bytes 131072 | tf_op jit(solution)/shard_map/all_to_all | solution.py:120
  162.0 1.3 convolution_convert_fusion
  163.4 0.5 all-gather.6.cloned.1.call-update
  163.9 0.1 reduce_sum.69
  164.0 0.1 copy.47
  164.2 0.1 select_reduce_fusion
  164.2 11.9 %reduce-scatter.7.cloned.1.call-done = bf16[8,8,512]{2,1,0:T(8,128)(2,1)} async-done(((bf16[8,8,2048]{2,1,0:T(8,128)(2,1)}), bf16[8,8,512]{2,1,0:T(8,128)(2,1)}) %reduce-scatter.7.cloned.1.call-update) | async-done | bytes 65552 | tf_op jit(solution)/shard_map/reduce_scatter | solution.py:101
  176.1 4.6 %all-to-all-start.2 = ((bf16[8,8,512]{2,1,0:T(8,128)(2,1)}), bf16[8,8,512]{2,1,0:T(8,128)(2,1)S(1)}, u32[]{:S(2)}, u32[]{:S(2)}) async-start(bf16[8,8,512]{2,1,0:T(8,128)(2,1)} %reduce-scatter.7.cloned.1.call-done), calls=%async_computation.4 | async-start | bytes 131072 | tf_op jit(solution)/shard_map/all_to_all | solution.py:104
  180.8 29.5 %reduce-scatter.9.cloned.1.call-done = bf16[16,3072]{1,0:T(8,128)(2,1)} async-done(((bf16[128,3072]{1,0:T(8,128)(2,1)}), bf16[16,3072]{1,0:T(8,128)(2,1)}) %reduce-scatter.9.cloned.1.call-update) | async-done | bytes 98320 | tf_op jit(solution)/shard_map/reduce_scatter | solution.py:121
  210.3 0.9 convert_element_type.82
  211.2 63.5 %all-gather.6.cloned.1.call-done = bf16[12288,256]{1,0:T(8,128)(2,1)} async-done(((bf16[1536,256]{1,0:T(8,128)(2,1)}), bf16[12288,256]{1,0:T(8,128)(2,1)}) %all-gather.6.cloned.1.call-update) | async-done | bytes 6291472 | tf_op jit(solution)/shard_map/all_gather | solution.py:129
  274.7 8.6 %copy.49 = bf16[1536,8,256]{0,2,1:T(8,128)(2,1)} copy(bf16[1536,8,256]{2,0,1:T(8,128)(2,1)} %bitcast.82) | data formatting | bytes 12582912 | tf_op jit(solution)/shard_map/reshape | solution.py:129
  283.4 5.1 %convolution_convert_fusion.3 = bf16[16,2048]{1,0:T(8,128)(2,1)} fusion(bf16[1536,2048]{0,1:T(8,128)(2,1)} %bitcast.81, f32[16,3072]{1,0:T(8,128)S(1)} %convert_element_type.82), kind=kOutput, calls=%fused_computation.12 | convolution fusion | flops 100843520 | bytes 6553600 | tf_op jit(solution)/shard_map/dot_general | solution.py:130
  288.5 0.1 fusion.22
  288.7 22.8 %reduce-scatter.11.cloned.1.call-done = bf16[16,512]{1,0:T(8,128)(2,1)} async-done(((bf16[16,2048]{1,0:T(8,128)(2,1)}), bf16[16,512]{1,0:T(8,128)(2,1)}) %reduce-scatter.11.cloned.1.call-update) | async-done | bytes 16400 | tf_op jit(solution)/shard_map/reduce_scatter | solution.py:133
  311.4 1.0 multiply_reduce_fusion.1
  312.4 8.9 %psum.15 = f32[16]{0:T(128)S(1)} all-reduce(f32[16]{0:T(128)S(1)} %get-tuple-element.14), channel_id=1, replica_groups=mesh['ep'=8,'tp'=4] {'tp'}, use_global_device_ids=true, to_apply=%region_13.14 | all-reduce | flops 16 | bytes 128 | tf_op jit(solution)/shard_map/psum | solution.py:138
  321.3 0.7 add_convert_fusion
  (51 shorter events, 0.7 us)
Async XLA Ops:
  7.2 18.1 %copy-start.4 = (s32[16,2]{0,1:T(2,128)S(1)}, s32[16,2]{0,1:T(2,128)}, u32[]{:S(2)}) copy-start(s32[16,2]{0,1:T(2,128)} %param.29) | copy-start | bytes 388
  7.2 18.6 %copy-start.2 = (f32[512]{0:T(512)S(1)}, f32[512]{0:T(512)}, u32[]{:S(2)}) copy-start(f32[512]{0:T(512)} %param.21) | copy-start | bytes 6148
  7.2 47.3 %reduce-scatter.5.cloned.1.call-start = ((), (), s32[]{:S(2)}) async-start(), calls=%async_computation.8 | async-start | bytes 589824 | tf_op jit(solution)/shard_map/reduce_scatter | solution.py:42
  24.5 60.5 %all-gather.4.cloned.1.call-start = ((), (), s32[]{:S(2)}) async-start(), calls=%async_computation.9 | async-start | bytes 2359296 | tf_op jit(solution)/shard_map/all_gather | solution.py:68
  25.2 103.5 %all-reduce.2.cloned.1.call-start = ((), (), s32[]{:S(2)}) async-start(), calls=%async_computation.10 | async-start | bytes 131072 | tf_op jit(solution)/shard_map/psum | solution.py:72
  60.6 2.0 copy-start
  60.6 5.8 %copy-start.5 = (f32[512]{0:T(512)S(1)}, f32[512]{0:T(512)}, u32[]{:S(2)}) copy-start(f32[512]{0:T(512)} %param.22) | copy-start | bytes 6148
  60.6 69.1 %copy-start.1 = (bf16[16,2048]{1,0:T(8,128)(2,1)S(1)}, bf16[16,2048]{1,0:T(8,128)(2,1)}, u32[]{:S(2)}) copy-start(bf16[16,2048]{1,0:T(8,128)(2,1)} %param.19) | copy-start | bytes 196612
  87.6 88.5 %reduce-scatter.7.cloned.1.call-start = ((), (), s32[]{:S(2)}) async-start(), calls=%async_computation.11 | async-start | bytes 327680 | tf_op jit(solution)/shard_map/reduce_scatter | solution.py:101
  148.1 13.9 %copy-start.7 = (bf16[256,1536]{1,0:T(8,128)(2,1)S(1)}, bf16[256,1536]{1,0:T(8,128)(2,1)}, u32[]{:S(2)}) copy-start(bf16[256,1536]{1,0:T(8,128)(2,1)} %param.35) | copy-start | bytes 2359300
  148.1 13.9 %copy-start.8 = (bf16[256,1536]{1,0:T(8,128)(2,1)S(1)}, bf16[256,1536]{1,0:T(8,128)(2,1)}, u32[]{:S(2)}) copy-start(bf16[256,1536]{1,0:T(8,128)(2,1)} %param.34) | copy-start | bytes 2359300
  153.6 10.3 %copy-start.3 = (bf16[2048]{0:T(1024)(128)(2,1)S(1)}, bf16[2048]{0:T(1024)(128)(2,1)}, u32[]{:S(2)}) copy-start(bf16[2048]{0:T(1024)(128)(2,1)} %param.37) | copy-start | bytes 12292
  153.6 10.5 %copy-start.6 = (f32[16,2]{0,1:T(2,128)S(1)}, f32[16,2]{0,1:T(2,128)}, u32[]{:S(2)}) copy-start(f32[16,2]{0,1:T(2,128)} %param.30) | copy-start | bytes 388
  153.7 56.6 %reduce-scatter.9.cloned.1.call-start = ((), (), s32[]{:S(2)}) async-start(), calls=%async_computation.12 | async-start | bytes 884736 | tf_op jit(solution)/shard_map/reduce_scatter | solution.py:121
  163.3 111.4 %all-gather.6.cloned.1.call-start = ((), (), s32[]{:S(2)}) async-start(), calls=%async_computation.14 | async-start | bytes 7077888 | tf_op jit(solution)/shard_map/all_gather | solution.py:129
  176.1 112.5 %all-to-all-start.2 = ((bf16[8,8,512]{2,1,0:T(8,128)(2,1)}), bf16[8,8,512]{2,1,0:T(8,128)(2,1)S(1)}, u32[]{:S(2)}, u32[]{:S(2)}) async-start(bf16[8,8,512]{2,1,0:T(8,128)(2,1)} %reduce-scatter.7.cloned.1.call-done), calls=%async_computation.4 | async-start | bytes 131072 | tf_op jit(solution)/shard_map/all_to_all | solution.py:104
  180.7 130.7 %reduce-scatter.11.cloned.1.call-start = ((), (), s32[]{:S(2)}) async-start(), calls=%async_computation.13 | async-start | bytes 81920 | tf_op jit(solution)/shard_map/reduce_scatter | solution.py:133
Sparse Core Ops, SparseCore 0:
  24.6 29.8 reduce-scatter.4
  56.1 28.8 all-gather.3
  87.9 40.8 all-reduce.1
  153.8 22.2 reduce-scatter.6
  178.2 31.9 reduce-scatter.8
  211.8 62.8 all-gather.5
  288.6 22.7 reduce-scatter.10
